TPU v7x, 32 devices: a whole 2x2x4 slice. The times are simulated.
32 devices in a mesh: sp: 8 (over z, y), tp: 4 (over x, core).
Axes of the slice: x: 2, y: 2, z: 4, core: 2. Of those that a mesh axis runs over, the one named last changes fastest.
Arguments:
- stream_in: bfloat16 [6144, 2048], P(('sp', 'tp')), may hold values from -6 to 6
- query_wide: bfloat16 [6144, 512], P('sp', 'tp'), may hold values from -6 to 6
- key_wide: bfloat16 [6144, 512], P('sp', 'tp'), may hold values from -6 to 6
- value_wide: bfloat16 [6144, 512], P('sp', 'tp'), may hold values from -6 to 6
- gate_wide: bfloat16 [6144, 512], P('sp', 'tp'), may hold values from -6 to 6
- decay_wide: float32 [4, 6144], P('tp', 'sp'), may hold values from -2.3 to 0, as said below
- query_narrow: bfloat16 [6144, 512], P('sp', 'tp'), may hold values from -6 to 6
- key_narrow: bfloat16 [6144, 512], P('sp', 'tp'), may hold values from -6 to 6
- value_narrow: bfloat16 [6144, 512], P('sp', 'tp'), may hold values from -6 to 6
- gate_narrow: bfloat16 [6144, 512], P('sp', 'tp'), may hold values from -6 to 6
- decay_narrow: float32 [8, 6144], P('tp', 'sp'), may hold values from -2.3 to 0, as said below
- output_wide: bfloat16 [512, 2048], P('tp'), may hold values from -0.25 to 0.25
- output_narrow: bfloat16 [512, 2048], P('tp'), may hold values from -0.25 to 0.25
- norm_gain: bfloat16 [2048], replicated, may hold values from 0.099609375 to 1.8984375
- up_weight: bfloat16 [2048, 8192], P('sp', 'tp'), may hold values from -0.125 to 0.125
- down_weight: bfloat16 [8192, 2048], P('tp', 'sp'), may hold values from -0.0625 to 0.0625
Outputs:
- layer_out: bfloat16 [6144, 2048], P(('sp', 'tp'))
Inputs may be any that keep to these rules, and one draw needn't show every extreme that they name: `decay_wide`: each entry is the logarithm of one head's retention factor at one position. `decay_narrow`: each entry is the logarithm of one head's retention factor at one position.
All inputs are finite; a program needn't handle non-finite values.
Results may differ from a plain program's by a relative error of at most 0.02.
Values may be sent and summed in bfloat16 or wider, within the bound.
A program may use at most 128 MiB of HBM per device.

v0:
```python
import jax
import jax.numpy as jnp
from jax import lax
from jax.sharding import PartitionSpec as P

HDW = 128
HDN = 64
BLOCK = 128
head_eps = 1e-05
norm_eps = 1e-06
rope_base = 10000.0


def carried_in(shard, axis, join, neutral):
    place = lax.axis_index(axis)
    gathered = jax.tree.map(
        lambda a, kind: lax.all_gather(a.astype(kind), axis),
        shard,
        (jnp.bfloat16, jnp.bfloat16, jnp.bfloat16, jnp.bfloat16),
    )
    state = jax.tree.map(lambda a, e: jnp.zeros_like(a) + jnp.asarray(e, a.dtype), shard, neutral)

    def one(turn, state):
        return join(
            state,
            jax.tree.map(
                lambda a, own: lax.dynamic_index_in_dim(a, turn, 0, False).astype(own.dtype),
                gathered,
                shard,
            ),
        )

    return lax.fori_loop(0, place, one, state)


def rotate(values, places):
    half = values.shape[-1] // 2
    inverse = rope_base ** (-jnp.arange(half, dtype=jnp.float32) / half)
    angles = places[:, None] * inverse[None, :]
    cosine = jnp.cos(angles)[:, None, :]
    sine = jnp.sin(angles)[:, None, :]
    front = values[..., :half]
    back = values[..., half:]
    return jnp.concatenate([front * cosine - back * sine, back * cosine + front * sine], axis=-1)


def block_step(carried, inputs):
    query, keys, values, log_rate = inputs
    running = jnp.cumsum(log_rate, axis=0)
    spread = running[:, None, :] - running[None, :, :]
    length = log_rate.shape[0]
    lower = (jnp.arange(length)[:, None] >= jnp.arange(length)[None, :])[:, :, None]
    factor = jnp.where(lower, jnp.exp(jnp.minimum(spread, 0.0)), 0.0)
    scores = jnp.einsum("thd,shd->tsh", query, keys) * factor
    within = jnp.einsum("tsh,she->the", scores, values)
    across = jnp.einsum("thd,hde->the", query, carried) * jnp.exp(running)[:, :, None]
    tail_decay = jnp.exp(running[-1][None, :] - running)
    updated = jnp.exp(running[-1])[:, None, None] * carried + jnp.einsum(
        "shd,she->hde", keys * tail_decay[:, :, None], values
    )
    return (updated, within + across)


def head_norm(values):
    centre = values - jnp.mean(values, axis=-1, keepdims=True)
    spread = jnp.mean(centre * centre, axis=-1, keepdims=True)
    return centre * lax.rsqrt(spread + head_eps)


def local_group(query, keys, values, log_rate, width, places):
    length = query.shape[0]
    count_of_heads = query.shape[1] // width
    blocks = length // BLOCK

    def split(array):
        return array.astype(jnp.float32).reshape(length, count_of_heads, width)

    query_rot = rotate(split(query), places)
    keys_rot = rotate(split(keys), places) * width ** (-0.5)
    rates = log_rate.T
    carried = jnp.zeros((count_of_heads, width, width), jnp.float32)
    final_state, outputs = lax.scan(
        block_step,
        carried,
        (
            query_rot.reshape(blocks, BLOCK, count_of_heads, width),
            keys_rot.reshape(blocks, BLOCK, count_of_heads, width),
            split(values).reshape(blocks, BLOCK, count_of_heads, width),
            rates.reshape(blocks, BLOCK, count_of_heads),
        ),
    )
    running = jnp.cumsum(rates, axis=0)
    return (
        query_rot,
        outputs.reshape(length, count_of_heads, width),
        final_state,
        jnp.exp(running[-1]),
        running,
    )


def finish_group(query_rot, outputs, incoming, running, gate):
    length = outputs.shape[0]
    outputs = (
        outputs + jnp.einsum("thd,hde->the", query_rot, incoming) * jnp.exp(running)[:, :, None]
    )
    normed = head_norm(outputs).reshape(length, -1)
    return (jax.nn.silu(gate.astype(jnp.float32)) * normed).astype(jnp.bfloat16)


def chain(earlier, later):
    rate_wide, memory_wide, rate_narrow, memory_narrow = earlier
    later_rate_wide, later_memory_wide, later_rate_narrow, later_memory_narrow = later
    return (
        rate_wide * later_rate_wide,
        memory_wide * later_rate_wide[:, None, None] + later_memory_wide,
        rate_narrow * later_rate_narrow,
        memory_narrow * later_rate_narrow[:, None, None] + later_memory_narrow,
    )


def row_norm(middle, norm_gain):
    middle_f = middle.astype(jnp.float32)
    scale = lax.rsqrt(jnp.mean(middle_f * middle_f, axis=-1, keepdims=True) + norm_eps)
    return (middle_f * scale * norm_gain.astype(jnp.float32)).astype(jnp.bfloat16)


def on_device(
    stream_in,
    query_wide,
    key_wide,
    value_wide,
    gate_wide,
    decay_wide,
    query_narrow,
    key_narrow,
    value_narrow,
    gate_narrow,
    decay_narrow,
    output_wide,
    output_narrow,
    norm_gain,
    up_weight,
    down_weight,
):
    length = query_wide.shape[0]
    places = (lax.axis_index("sp") * length + jnp.arange(length, dtype=jnp.int32)).astype(
        jnp.float32
    )
    wide_query, wide_out, wide_state, wide_total, wide_running = local_group(
        query_wide, key_wide, value_wide, decay_wide, HDW, places
    )
    narrow_query, narrow_out, narrow_state, narrow_total, narrow_running = local_group(
        query_narrow, key_narrow, value_narrow, decay_narrow, HDN, places
    )
    identity = (
        jnp.ones_like(wide_total),
        jnp.zeros_like(wide_state),
        jnp.ones_like(narrow_total),
        jnp.zeros_like(narrow_state),
    )
    incoming = carried_in(
        (wide_total, wide_state, narrow_total, narrow_state), "sp", chain, identity
    )
    mixed_wide = finish_group(wide_query, wide_out, incoming[1], wide_running, gate_wide)
    mixed_narrow = finish_group(narrow_query, narrow_out, incoming[3], narrow_running, gate_narrow)
    mixed_sum = lax.psum_scatter(
        (
            jnp.dot(mixed_wide, output_wide, preferred_element_type=jnp.float32)
            + jnp.dot(mixed_narrow, output_narrow, preferred_element_type=jnp.float32)
        ).astype(jnp.bfloat16),
        "tp",
        scatter_dimension=0,
        tiled=True,
    ).astype(jnp.float32)
    middle = (stream_in.astype(jnp.float32) + mixed_sum).astype(jnp.bfloat16)
    normed = lax.all_gather(row_norm(middle, norm_gain), "tp", axis=0, tiled=True)
    up_sum = jnp.dot(
        normed,
        lax.all_gather(up_weight, "sp", axis=0, tiled=True),
        preferred_element_type=jnp.float32,
    )
    hidden = jnp.square(jax.nn.relu(up_sum)).astype(jnp.bfloat16)
    down_sum = jnp.dot(
        hidden,
        lax.all_gather(down_weight, "sp", axis=1, tiled=True),
        preferred_element_type=jnp.float32,
    )
    down_rows = lax.psum_scatter(
        down_sum.astype(jnp.bfloat16), "tp", scatter_dimension=0, tiled=True
    ).astype(jnp.float32)
    return (middle.astype(jnp.float32) + down_rows).astype(jnp.bfloat16)


def solution(mesh):
    in_specs = (
        P(("sp", "tp"), None),
        P("sp", "tp"),
        P("sp", "tp"),
        P("sp", "tp"),
        P("sp", "tp"),
        P("tp", "sp"),
        P("sp", "tp"),
        P("sp", "tp"),
        P("sp", "tp"),
        P("sp", "tp"),
        P("tp", "sp"),
        P("tp", None),
        P("tp", None),
        P(),
        P("sp", "tp"),
        P("tp", "sp"),
    )
    out_specs = P(("sp", "tp"), None)
    return jax.shard_map(
        on_device, mesh=mesh, in_specs=in_specs, out_specs=out_specs, check_vma=False
    )
```

profile of v0, /device:TPU:0, one launch (start us, length us, event | category | flops | bytes accessed | tf_op | source)
XLA Modules:
  0.0 578.7 jit_solution(15378131517314459082)
XLA Ops:
  6.6 0.8 reduce.3
  8.2 1.1 copy.75
  9.3 1.1 copy.77
  11.9 25.0 %while.43 = (s32[]{:T(128)}, f32[2,64,64]{2,1,0:T(8,128)S(1)}, f32[6,128,2,64]{1,0,3,2:T(8,128)}, f32[6,128,2]{2,1,0:T(8,128)S(1)}, f32[6,128,2,64]{1,0,3,2:T(8,...) while((s32[]{:T(128)}, f32[2,64,64]{2,1,0:T(8,128)S(1)}, ...), condition=%wide.region_9.10_spmd.clone, body=%wide.region_7.9_spmd.clone.sunk | while | flops 12877827 | bytes 1099440 | solution.py:82
  13.0 2.8 dynamic_update_slice.14
  17.2 2.8 dynamic_update_slice.14
  21.4 2.8 dynamic_update_slice.14
  25.5 2.8 dynamic_update_slice.14
  29.7 2.8 dynamic_update_slice.14
  33.8 2.8 dynamic_update_slice.14
  36.9 34.6 %all-gather.1 = bf16[16,64,64]{2,1,0:T(8,128)(2,1)} all-gather(bf16[2,64,64]{2,1,0:T(8,128)(2,1)S(1)} %convert_element_type.115), channel_id=3, replica_groups=mesh['sp'=8,'tp'=4] {'sp'}, dimensions={0}, use_global_device_ids=true | all-gather | bytes 147456 | tf_op jit(solution)/shard_map/all_gather | solution.py:17
  71.4 1.0 reshape_reshape.16
  72.4 1.0 bitcast_convert_fusion.1
  73.4 1.9 fusion.74
  75.4 0.9 maximum_multiply_fusion.1
  76.4 27.8 %while.42 = (s32[]{:T(128)}, f32[1,128,128]{2,1,0:T(8,128)S(1)}, f32[6,128,1,128]{3,1,0,2:T(8,128)}, f32[6,128,1]{1,2,0:T(1,128)}, f32[6,128,1,128]{3,2,1,0:T(1,...) while((s32[]{:T(128)}, f32[1,128,128]{2,1,0:T(8,128)S(1)}, ...), condition=%wide.region_2.3_spmd.clone, body=%wide.region_0.2_spmd.clone.sunk | while | flops 17006596 | bytes 1515172 | solution.py:82
  76.4 0.7 fusion.149
  78.0 0.6 fusion.150
  81.0 0.7 fusion.149
  82.6 0.6 fusion.150
  85.6 0.7 fusion.149
  87.2 0.6 fusion.150
  90.3 0.7 fusion.149
  91.9 0.6 fusion.150
  94.9 0.7 fusion.149
  96.5 0.6 fusion.150
  99.5 0.7 fusion.149
  101.1 0.6 fusion.150
  102.6 0.6 constant_dynamic-update-slice_fusion.2
  104.2 30.9 %all-gather = bf16[8,128,128]{2,1,0:T(8,128)(2,1)S(1)} all-gather(bf16[1,128,128]{2,1,0:T(8,128)(2,1)S(1)} %convert_element_type.113), channel_id=2, replica_groups=mesh['sp'=8,'tp'=4] {'sp'}, dimensions={0}, use_global_device_ids=true | all-gather | bytes 294912 | tf_op jit(solution)/shard_map/all_gather | solution.py:17
  135.7 0.6 slice.73
  138.3 0.7 dynamic-update-slice
  139.0 21.4 %all-reduce = bf16[8]{0:T(256)(128)(2,1)S(1)} all-reduce(bf16[8]{0:T(256)(128)(2,1)S(1)} %dynamic-update-slice), channel_id=1, replica_groups=mesh['sp'=8,'tp'=4] {'sp'}, use_global_device_ids=true, to_apply=%add | all-reduce | flops 8 | bytes 32
  161.6 16.3 %all-gather.2 = bf16[8,1,2]{2,1,0:T(2,128)(2,1)S(1)} all-gather(bf16[1,1,2]{2,1,0:T(2,128)(2,1)S(1)} %bitcast.321), channel_id=1, replica_groups=mesh['sp'=8,'tp'=4] {'sp'}, dimensions={0}, use_global_device_ids=true | all-gather | bytes 36 | tf_op jit(solution)/shard_map/all_gather | solution.py:17
  178.0 1.2 reshape.610
  180.7 1.0 fusion.79
  181.7 2.7 add_convert_fusion
  185.1 52.4 %reduce-scatter.3.cloned.1.call-done = bf16[192,2048]{1,0:T(8,128)(2,1)} async-done(((bf16[768,2048]{1,0:T(8,128)(2,1)}), bf16[192,2048]{1,0:T(8,128)(2,1)}) %reduce-scatter.3.cloned.1.call-update) | async-done | bytes 786448 | tf_op jit(solution)/shard_map/reduce_scatter | solution.py:167
  237.5 1.5 fusion.47
  239.0 2.3 fusion.49
  241.4 0.7 all-gather.9.cloned.1.call-update
  242.9 27.1 %all-gather.7.cloned.1.call-done = bf16[768,2048]{1,0:T(8,128)(2,1)} async-done(((bf16[192,2048]{1,0:T(8,128)(2,1)}), bf16[768,2048]{1,0:T(8,128)(2,1)}) %all-gather.7.cloned.1.call-update) | async-done | bytes 3145744 | tf_op jit(solution)/shard_map/all_gather | solution.py:177
  270.0 126.6 %all-gather.9.cloned.1.call-done = bf16[2048,2048]{1,0:T(8,128)(2,1)} async-done(((bf16[256,2048]{1,0:T(8,128)(2,1)}), bf16[2048,2048]{1,0:T(8,128)(2,1)}) %all-gather.9.cloned.1.call-update) | async-done | bytes 8388624 | tf_op jit(solution)/shard_map/all_gather | solution.py:180
  396.7 11.9 %multiply_convert_fusion = bf16[768,2048]{1,0:T(8,128)(2,1)} fusion(bf16[768,2048]{1,0:T(8,128)(2,1)} %all-gather.7.cloned.1.call-done, bf16[2048,2048]{1,0:T(8,128)(2,1)} %all-gather.9.cloned.1.call-done), kind=kOutput, calls=%fused_computation.73 | convolution fusion | flops 6447169536 | bytes 14680064 | tf_op jit(solution)/shard_map/dot_general | solution.py:178
  408.5 113.2 %all-gather.11.cloned.1.call-done = bf16[2048,2048]{1,0:T(8,128)(2,1)} async-done(((bf16[2048,256]{1,0:T(8,128)(2,1)}), bf16[2048,2048]{1,0:T(8,128)(2,1)}) %all-gather.11.cloned.1.call-update) | async-done | bytes 8388624 | tf_op jit(solution)/shard_map/all_gather | solution.py:186
  521.7 11.9 %convolution_convert_fusion = bf16[768,2048]{1,0:T(8,128)(2,1)} fusion(bf16[768,2048]{1,0:T(8,128)(2,1)} %multiply_convert_fusion, bf16[2048,2048]{1,0:T(8,128)(2,1)} %all-gather.11.cloned.1.call-done), kind=kOutput, calls=%fused_computation.75 | convolution fusion | flops 6444023808 | bytes 14680064 | tf_op jit(solution)/shard_map/dot_general | solution.py:184
  533.6 36.2 %reduce-scatter.5.cloned.1.call-done = bf16[192,2048]{1,0:T(8,128)(2,1)} async-done(((bf16[768,2048]{1,0:T(8,128)(2,1)}), bf16[192,2048]{1,0:T(8,128)(2,1)}) %reduce-scatter.5.cloned.1.call-update) | async-done | bytes 786448 | tf_op jit(solution)/shard_map/reduce_scatter | solution.py:189
  569.8 2.4 fusion.50
  (233 shorter events, 30.5 us)
Async XLA Ops:
  6.5 174.1 %copy-start = (bf16[128,2048]{1,0:T(8,128)(2,1)S(1)}, bf16[128,2048]{1,0:T(8,128)(2,1)}, u32[]{:S(2)}) copy-start(bf16[128,2048]{1,0:T(8,128)(2,1)} %param.33) | copy-start | bytes 1572868
  6.5 4.5 copy-start.8
  6.5 231.0 %reduce-scatter.3.cloned.1.call-start = ((), (), s32[]{:S(2)}) async-start(), calls=%async_computation.2 | async-start | bytes 3932160 | tf_op jit(solution)/shard_map/reduce_scatter | solution.py:167
  9.3 2.3 copy-start.9
  11.9 60.5 %copy-start.5 = (bf16[768,128]{1,0:T(8,128)(2,1)S(1)}, bf16[768,128]{1,0:T(8,128)(2,1)}, u32[]{:S(2)}) copy-start(bf16[768,128]{1,0:T(8,128)(2,1)} %param.23) | copy-start | bytes 589828
  76.4 61.3 %copy-start.11 = (u32[32]{0:T(128)S(1)}, u32[32]{0:T(128)}, u32[]{:S(2)}) copy-start(u32[32]{0:T(128)} %constant.123) | copy-start | bytes 388
  104.2 75.5 %copy-start.6 = (bf16[768,128]{1,0:T(8,128)(2,1)S(1)}, bf16[768,128]{1,0:T(8,128)(2,1)}, u32[]{:S(2)}) copy-start(bf16[768,128]{1,0:T(8,128)(2,1)} %param.31) | copy-start | bytes 589828
  104.2 75.6 %copy-start.4 = (f32[6,128,1,128]{3,1,0,2:T(8,128)S(1)}, f32[6,128,1,128]{3,1,0,2:T(8,128)}, u32[]{:S(2)}) copy-start(f32[6,128,1,128]{3,1,0,2:T(8,128)} %get-tuple-element.151) | copy-start | bytes 1179652
  178.0 2.4 copy-start.7
  180.7 1.0 copy-start.3
  184.4 0.7 copy-start.10
  184.4 53.1 %copy-start.1 = (bf16[192,2048]{1,0:T(8,128)(2,1)S(1)}, bf16[192,2048]{1,0:T(8,128)(2,1)}, u32[]{:S(2)}) copy-start(bf16[192,2048]{1,0:T(8,128)(2,1)} %param.22) | copy-start | bytes 2359300
  184.4 85.6 %all-gather.7.cloned.1.call-start = ((), (), s32[]{:S(2)}) async-start(), calls=%async_computation.3 | async-start | bytes 3932160 | tf_op jit(solution)/shard_map/all_gather | solution.py:177
  241.3 155.3 %all-gather.9.cloned.1.call-start = ((), (), s32[]{:S(2)}) async-start(), calls=%async_computation.4 | async-start | bytes 9437184 | tf_op jit(solution)/shard_map/all_gather | solution.py:180
  242.1 279.6 %all-gather.11.cloned.1.call-start = ((), (), s32[]{:S(2)}) async-start(), calls=%async_computation.5 | async-start | bytes 9437184 | tf_op jit(solution)/shard_map/all_gather | solution.py:186
  242.7 327.2 %reduce-scatter.5.cloned.1.call-start = ((), (), s32[]{:S(2)}) async-start(), calls=%async_computation.6 | async-start | bytes 3932160 | tf_op jit(solution)/shard_map/reduce_scatter | solution.py:189
  533.6 36.2 %copy-start.2 = (bf16[192,2048]{1,0:T(8,128)(2,1)S(1)}, bf16[192,2048]{1,0:T(8,128)(2,1)}, u32[]{:S(2)}) copy-start(bf16[192,2048]{1,0:T(8,128)(2,1)} %reduce-scatter.3.cloned.1.call-done) | copy-start | bytes 2359300
Sparse Core Ops, SparseCore 0:
  184.5 52.9 reduce-scatter.2
  241.5 28.5 all-gather.6
  272.1 124.4 all-gather.8
  398.6 123.1 all-gather.10
  533.7 36.0 reduce-scatter.4
where the time goes:
time: 580 us; the launch traced here: 579 us
  waiting for transfers between devices  357 us (62%)
  blocking collectives  103 us (18%)
  local copies, waits for them, and re-layouts  39.6 us (7%)
  matrix products  36.5 us (6%)
  other arithmetic  22.5 us (4%)
  between operations  14.9 us (3%)
    all_gather x1, waiting for transfers between devices, on_device(): lax.all_gather(up_weight, 'sp', axis=0, tiled=True)  127 us
    all_gather x1, waiting for transfers between devices, on_device(): lax.all_gather(down_weight, 'sp', axis=1, tiled=True)  113 us
    all_gather x3, blocking collectives, carried_in(): lax.all_gather(a.astype(kind), axis)  81.7 us
    reduce_scatter x1, waiting for transfers between devices, on_device(): lax.psum_scatter((jnp.dot(mixed_wide, output_wide, preferred_element_type...  52.4 us
    reduce_scatter x1, waiting for transfers between devices, on_device(): lax.psum_scatter(down_sum.astype(jnp.bfloat16), 'tp', scatter_dimension=0...  36.2 us
    all_gather x1, waiting for transfers between devices, on_device(): lax.all_gather(row_norm(middle, norm_gain), 'tp', axis=0, tiled=True)  27.1 us
    unnamed x1, blocking collectives  21.4 us
    dynamic_update_slice x18, local copies, waits for them, and re-layouts, local_group(): lax.scan(block_step, carried, (query_rot.reshape(blocks, BLOCK, count_of_...  21.1 us
  transfers between devices with their start and end apart: 5, of which 5 were waited for; matrix products, arithmetic and copies ran while one was open for 2% of the time, Pallas kernels for 0%

commit v1 on v0

--- a/solution.py
+++ b/solution.py
@@ -177,7 +177,9 @@
     normed = lax.all_gather(row_norm(middle, norm_gain), "tp", axis=0, tiled=True)
     up_sum = jnp.dot(
         normed,
-        lax.all_gather(up_weight, "sp", axis=0, tiled=True),
+        jnp.concatenate(
+            lax.all_to_all(jnp.stack([up_weight] * lax.axis_size("sp")), "sp", 0, 0), axis=0
+        ),
         preferred_element_type=jnp.float32,
     )
     hidden = jnp.square(jax.nn.relu(up_sum)).astype(jnp.bfloat16)

time: 580 us -> 606 us (1.045)
  waiting for transfers between devices: 357 us -> 373 us
    all_to_all x0 -> x1, waiting for transfers between devices: none -> 265 us  [on_device(): lax.all_to_all(jnp.stack([up_weight] * lax.axis_size('sp')), 'sp', 0, 0)]
    all_gather x1 -> x0, waiting for transfers between devices: 127 us -> none  [on_device(): lax.all_gather(up_weight, 'sp', axis=0, tiled=True)]
    all_gather x1, waiting for transfers between devices: 113 us -> 0.01 us  [on_device(): lax.all_gather(down_weight, 'sp', axis=1, tiled=True)]
    all_gather x1, waiting for transfers between devices: 27.1 us -> 17.9 us  [on_device(): lax.all_gather(row_norm(middle, norm_gain), 'tp', axis=0, tiled=True)]
  transfers between devices with their start and end apart: 5 -> 5, of which waited for: 5 -> 4; matrix products, arithmetic and copies ran while one was open for 2% -> 3% of each run, Pallas kernels for 0% -> 0%
where the time goes in v1:
time: 606 us; the launch traced here: 604 us
  waiting for transfers between devices  373 us (62%)
  blocking collectives  103 us (17%)
  local copies, waits for them, and re-layouts  43.9 us (7%)
  matrix products  36.5 us (6%)
  other arithmetic  22.5 us (4%)
  between operations  14.9 us (2%)
    all_to_all x1, waiting for transfers between devices, on_device(): lax.all_to_all(jnp.stack([up_weight] * lax.axis_size('sp')), 'sp', 0, 0)  265 us
    all_gather x3, blocking collectives, carried_in(): lax.all_gather(a.astype(kind), axis)  81.7 us
    reduce_scatter x1, waiting for transfers between devices, on_device(): lax.psum_scatter((jnp.dot(mixed_wide, output_wide, preferred_element_type...  52.4 us
    reduce_scatter x1, waiting for transfers between devices, on_device(): lax.psum_scatter(down_sum.astype(jnp.bfloat16), 'tp', scatter_dimension=0...  36.1 us
    unnamed x1, blocking collectives  21.4 us
    dynamic_update_slice x18, local copies, waits for them, and re-layouts, local_group(): lax.scan(block_step, carried, (query_rot.reshape(blocks, BLOCK, count_of_...  21.1 us
    all_gather x1, waiting for transfers between devices, on_device(): lax.all_gather(row_norm(middle, norm_gain), 'tp', axis=0, tiled=True)  17.9 us
  transfers between devices with their start and end apart: 5, of which 4 were waited for; matrix products, arithmetic and copies ran while one was open for 3% of the time, Pallas kernels for 0%

profile of v1, /device:TPU:0, one launch (start us, length us, event | category | flops | bytes accessed | tf_op | source)
XLA Modules:
  0.0 604.2 jit_solution(15004428358241494088)
XLA Ops:
  6.6 0.8 reduce.3
  8.2 1.1 copy.75
  9.3 1.1 copy.77
  11.9 25.0 %while.43 = (s32[]{:T(128)}, f32[2,64,64]{2,1,0:T(8,128)S(1)}, f32[6,128,2,64]{1,0,3,2:T(8,128)}, f32[6,128,2]{2,1,0:T(8,128)S(1)}, f32[6,128,2,64]{1,0,3,2:T(8,...) while((s32[]{:T(128)}, f32[2,64,64]{2,1,0:T(8,128)S(1)}, ...), condition=%wide.region_9.10_spmd.clone, body=%wide.region_7.9_spmd.clone.sunk | while | flops 12877827 | bytes 1099440 | solution.py:82
  13.0 2.8 dynamic_update_slice.14
  17.2 2.8 dynamic_update_slice.14
  21.4 2.8 dynamic_update_slice.14
  25.5 2.8 dynamic_update_slice.14
  29.7 2.8 dynamic_update_slice.14
  33.8 2.8 dynamic_update_slice.14
  36.9 34.6 %all-gather.1 = bf16[16,64,64]{2,1,0:T(8,128)(2,1)} all-gather(bf16[2,64,64]{2,1,0:T(8,128)(2,1)S(1)} %convert_element_type.115), channel_id=3, replica_groups=mesh['sp'=8,'tp'=4] {'sp'}, dimensions={0}, use_global_device_ids=true | all-gather | bytes 147456 | tf_op jit(solution)/shard_map/all_gather | solution.py:17
  71.4 1.0 reshape_reshape.16
  72.4 1.0 bitcast_convert_fusion.1
  73.4 1.9 fusion.74
  75.4 0.9 maximum_multiply_fusion.1
  76.4 27.8 %while.42 = (s32[]{:T(128)}, f32[1,128,128]{2,1,0:T(8,128)S(1)}, f32[6,128,1,128]{3,1,0,2:T(8,128)}, f32[6,128,1]{1,2,0:T(1,128)}, f32[6,128,1,128]{3,2,1,0:T(1,...) while((s32[]{:T(128)}, f32[1,128,128]{2,1,0:T(8,128)S(1)}, ...), condition=%wide.region_2.3_spmd.clone, body=%wide.region_0.2_spmd.clone.sunk | while | flops 17006596 | bytes 1515172 | solution.py:82
  76.4 0.7 fusion.149
  78.0 0.6 fusion.150
  81.0 0.7 fusion.149
  82.6 0.6 fusion.150
  85.6 0.7 fusion.149
  87.2 0.6 fusion.150
  90.3 0.7 fusion.149
  91.9 0.6 fusion.150
  94.9 0.7 fusion.149
  96.5 0.6 fusion.150
  99.5 0.7 fusion.149
  101.1 0.6 fusion.150
  102.6 0.6 constant_dynamic-update-slice_fusion.2
  104.2 30.9 %all-gather = bf16[8,128,128]{2,1,0:T(8,128)(2,1)S(1)} all-gather(bf16[1,128,128]{2,1,0:T(8,128)(2,1)S(1)} %convert_element_type.113), channel_id=2, replica_groups=mesh['sp'=8,'tp'=4] {'sp'}, dimensions={0}, use_global_device_ids=true | all-gather | bytes 294912 | tf_op jit(solution)/shard_map/all_gather | solution.py:17
  138.3 0.7 dynamic-update-slice
  139.0 21.4 %all-reduce = bf16[8]{0:T(256)(128)(2,1)S(1)} all-reduce(bf16[8]{0:T(256)(128)(2,1)S(1)} %dynamic-update-slice), channel_id=1, replica_groups=mesh['sp'=8,'tp'=4] {'sp'}, use_global_device_ids=true, to_apply=%add | all-reduce | flops 8 | bytes 32
  161.6 16.3 %all-gather.2 = bf16[8,1,2]{2,1,0:T(2,128)(2,1)S(1)} all-gather(bf16[1,1,2]{2,1,0:T(2,128)(2,1)S(1)} %bitcast.322), channel_id=1, replica_groups=mesh['sp'=8,'tp'=4] {'sp'}, dimensions={0}, use_global_device_ids=true | all-gather | bytes 36 | tf_op jit(solution)/shard_map/all_gather | solution.py:17
  178.0 1.2 reshape.615
  180.7 1.0 fusion.79
  181.7 2.7 add_convert_fusion
  185.1 52.4 %reduce-scatter.3.cloned.1.call-done = bf16[192,2048]{1,0:T(8,128)(2,1)} async-done(((bf16[768,2048]{1,0:T(8,128)(2,1)}), bf16[192,2048]{1,0:T(8,128)(2,1)}) %reduce-scatter.3.cloned.1.call-update) | async-done | bytes 786448 | tf_op jit(solution)/shard_map/reduce_scatter | solution.py:167
  237.5 1.5 fusion.47
  239.0 2.3 fusion.49
  241.4 4.3 stack.2
  245.6 5.5 all-to-all-start
  251.2 0.7 all-gather.8.cloned.1.call-update
  252.1 17.9 %all-gather.6.cloned.1.call-done = bf16[768,2048]{1,0:T(8,128)(2,1)} async-done(((bf16[192,2048]{1,0:T(8,128)(2,1)}), bf16[768,2048]{1,0:T(8,128)(2,1)}) %all-gather.6.cloned.1.call-update) | async-done | bytes 3145744 | tf_op jit(solution)/shard_map/all_gather | solution.py:177
  270.0 265.3 %all-to-all-done = bf16[8,256,2048]{2,1,0:T(8,128)(2,1)} async-done(((bf16[8,256,2048]{2,1,0:T(8,128)(2,1)}), bf16[8,256,2048]{2,1,0:T(8,128)(2,1)}, u32[]{:S(2)}, u32[]{:S(2)}) %all-to-all-start) | async-done | bytes 8388640 | tf_op jit(solution)/shard_map/all_to_all | solution.py:181
  535.4 11.9 %multiply_convert_fusion = bf16[768,2048]{1,0:T(8,128)(2,1)} fusion(bf16[768,2048]{1,0:T(8,128)(2,1)} %all-gather.6.cloned.1.call-done, bf16[2048,2048]{1,0:T(8,128)(2,1)} %bitcast.36), kind=kOutput, calls=%fused_computation.73 | convolution fusion | flops 6447169536 | bytes 14680064 | tf_op jit(solution)/shard_map/dot_general | solution.py:178
  547.2 11.9 %convolution_convert_fusion = bf16[768,2048]{1,0:T(8,128)(2,1)} fusion(bf16[768,2048]{1,0:T(8,128)(2,1)} %multiply_convert_fusion, bf16[2048,2048]{1,0:T(8,128)(2,1)} %all-gather.8.cloned.1.call-done), kind=kOutput, calls=%fused_computation.75 | convolution fusion | flops 6444023808 | bytes 14680064 | tf_op jit(solution)/shard_map/dot_general | solution.py:186
  559.1 36.1 %reduce-scatter.5.cloned.1.call-done = bf16[192,2048]{1,0:T(8,128)(2,1)} async-done(((bf16[768,2048]{1,0:T(8,128)(2,1)}), bf16[192,2048]{1,0:T(8,128)(2,1)}) %reduce-scatter.5.cloned.1.call-update) | async-done | bytes 786448 | tf_op jit(solution)/shard_map/reduce_scatter | solution.py:191
  595.2 2.4 fusion.50
  (235 shorter events, 30.5 us)
Async XLA Ops:
  6.5 174.1 %copy-start = (bf16[128,2048]{1,0:T(8,128)(2,1)S(1)}, bf16[128,2048]{1,0:T(8,128)(2,1)}, u32[]{:S(2)}) copy-start(bf16[128,2048]{1,0:T(8,128)(2,1)} %param.33) | copy-start | bytes 1572868
  6.5 4.5 copy-start.9
  6.5 231.0 %reduce-scatter.3.cloned.1.call-start = ((), (), s32[]{:S(2)}) async-start(), calls=%async_computation.3 | async-start | bytes 3932160 | tf_op jit(solution)/shard_map/reduce_scatter | solution.py:167
  9.3 2.3 copy-start.10
  11.9 60.5 %copy-start.6 = (bf16[768,128]{1,0:T(8,128)(2,1)S(1)}, bf16[768,128]{1,0:T(8,128)(2,1)}, u32[]{:S(2)}) copy-start(bf16[768,128]{1,0:T(8,128)(2,1)} %param.23) | copy-start | bytes 589828
  76.4 61.3 %copy-start.12 = (u32[32]{0:T(128)S(1)}, u32[32]{0:T(128)}, u32[]{:S(2)}) copy-start(u32[32]{0:T(128)} %constant.123) | copy-start | bytes 388
  104.2 75.5 %copy-start.7 = (bf16[768,128]{1,0:T(8,128)(2,1)S(1)}, bf16[768,128]{1,0:T(8,128)(2,1)}, u32[]{:S(2)}) copy-start(bf16[768,128]{1,0:T(8,128)(2,1)} %param.31) | copy-start | bytes 589828
  104.2 75.6 %copy-start.5 = (f32[6,128,1,128]{3,1,0,2:T(8,128)S(1)}, f32[6,128,1,128]{3,1,0,2:T(8,128)}, u32[]{:S(2)}) copy-start(f32[6,128,1,128]{3,1,0,2:T(8,128)} %get-tuple-element.151) | copy-start | bytes 1179652
  178.0 2.4 copy-start.8
  180.7 1.0 copy-start.4
  184.4 0.7 copy-start.11
  184.4 53.1 %copy-start.1 = (bf16[192,2048]{1,0:T(8,128)(2,1)S(1)}, bf16[192,2048]{1,0:T(8,128)(2,1)}, u32[]{:S(2)}) copy-start(bf16[192,2048]{1,0:T(8,128)(2,1)} %param.22) | copy-start | bytes 2359300
  184.4 56.9 %copy-start.3 = (bf16[256,2048]{1,0:T(8,128)(2,1)S(1)}, bf16[256,2048]{1,0:T(8,128)(2,1)}, u32[]{:S(2)}) copy-start(bf16[256,2048]{1,0:T(8,128)(2,1)} %param.36) | copy-start | bytes 3145732
  184.4 85.6 %all-gather.6.cloned.1.call-start = ((), (), s32[]{:S(2)}) async-start(), calls=%async_computation.4 | async-start | bytes 3932160 | tf_op jit(solution)/shard_map/all_gather | solution.py:177
  245.6 289.7 %all-to-all-start = ((bf16[8,256,2048]{2,1,0:T(8,128)(2,1)}), bf16[8,256,2048]{2,1,0:T(8,128)(2,1)}, u32[]{:S(2)}, u32[]{:S(2)}) async-start(bf16[8,256,2048]{2,1,0:T(8,128)(2,1)} %stack.2), calls=%async_computation.1 | async-start | bytes 16777216 | tf_op jit(solution)/shard_map/all_to_all | solution.py:181
  251.2 296.1 %all-gather.8.cloned.1.call-start = ((), (), s32[]{:S(2)}) async-start(), calls=%async_computation.5 | async-start | bytes 9437184 | tf_op jit(solution)/shard_map/all_gather | solution.py:188
  251.9 343.3 %reduce-scatter.5.cloned.1.call-start = ((), (), s32[]{:S(2)}) async-start(), calls=%async_computation.6 | async-start | bytes 3932160 | tf_op jit(solution)/shard_map/reduce_scatter | solution.py:191
  559.1 36.2 %copy-start.2 = (bf16[192,2048]{1,0:T(8,128)(2,1)S(1)}, bf16[192,2048]{1,0:T(8,128)(2,1)}, u32[]{:S(2)}) copy-start(bf16[192,2048]{1,0:T(8,128)(2,1)} %reduce-scatter.3.cloned.1.call-done) | copy-start | bytes 2359300
Sparse Core Ops, SparseCore 0:
  184.5 52.9 reduce-scatter.2
  241.5 28.5 all-gather.5
  272.1 263.2 all-gather.7
  559.2 35.9 reduce-scatter.4
